TPU v7x, 256 devices: a whole 4x4x8 slice. The times are simulated.
256 devices in a mesh: sp: 32 (over z, x), tp: 8 (over y, core).
Axes of the slice: x: 4, y: 4, z: 8, core: 2. Of those that a mesh axis runs over, the one named last changes fastest.
Arguments:
- broad_probe_tensor: bfloat16 [16384, 1024], P('sp', 'tp'), may hold values from -6 to 6
- broad_lookup_tensor: bfloat16 [16384, 1024], P('sp', 'tp'), may hold values from -6 to 6
- broad_payload_tensor: bfloat16 [16384, 1024], P('sp', 'tp'), may hold values from -6 to 6
- broad_emission_valve: bfloat16 [16384, 1024], P('sp', 'tp'), may hold values from -6 to 6
- slim_probe_tensor: bfloat16 [16384, 1024], P('sp', 'tp'), may hold values from -6 to 6
- slim_lookup_tensor: bfloat16 [16384, 1024], P('sp', 'tp'), may hold values from -6 to 6
- slim_payload_tensor: bfloat16 [16384, 1024], P('sp', 'tp'), may hold values from -6 to 6
- slim_emission_valve: bfloat16 [16384, 1024], P('sp', 'tp'), may hold values from -6 to 6
- broad_forgetting_speed: float32 [8], P('tp'), may hold values from -0.08 to 0
- slim_forgetting_speed: float32 [16], P('tp'), may hold values from -0.08 to 0
- broad_channel_scaling: float32 [1024], P('tp'), may hold values from 0.1 to 1.9
- slim_channel_scaling: float32 [1024], P('tp'), may hold values from 0.1 to 1.9
- surge_forgetting: float32 [16384], P('sp'), may hold values from -2.1 to 0
- broad_emission_proj: bfloat16 [1024, 2048], replicated, may hold values from -0.125 to 0.125
- slim_emission_proj: bfloat16 [1024, 2048], replicated, may hold values from -0.125 to 0.125
- skip_stream: bfloat16 [16384, 2048], P(('sp', 'tp')), may hold values from -6 to 6
- premix_scaling_coeffs: float32 [2048], replicated, may hold values from 0.1 to 1.9
- routed_specialist_ids: int32 [16384, 2], P('sp'), may hold values from 0 to 31, as said below
- routed_specialist_shares: float32 [16384, 2], P('sp'), may hold values from 0.2 to 1
- specialist_valve_proj: bfloat16 [32, 2048, 2048], P('sp', None, 'tp'), may hold values from -0.125 to 0.125
- specialist_expand_proj: bfloat16 [32, 2048, 2048], P('sp', None, 'tp'), may hold values from -0.125 to 0.125
- specialist_contract_proj: bfloat16 [32, 2048, 2048], P('sp', 'tp'), may hold values from -0.125 to 0.125
Outputs:
- result: bfloat16 [16384, 2048], P(('sp', 'tp'))
Inputs may be any that keep to these rules, and one draw needn't show every extreme that they name: `routed_specialist_ids`: each row names two different experts of one group, that is of the same run of 8 consecutive experts. The rows of one device (each aligned block of 64 rows) name each expert at most 8 times, and some expert is named exactly 8 times by the rows of every device.
All inputs are finite; a program needn't handle non-finite values.
Results may differ from a plain program's by a relative error of at most 0.018.
Values may be sent and summed in bfloat16 or wider, within the bound.
A program may use at most 128 MiB of HBM per device.

v0:
```python
import jax
import jax.numpy as jnp
from jax import lax
from jax.sharding import Mesh
from jax.sharding import PartitionSpec as P

BROAD_CHANNEL_DIM = 128
THIN_CHANNEL_DIM = 64
GROUPS = 4
SP = ("sp_0", "sp_1")
SP_TP = ("sp_0", "sp_1", "tp")
rope_base = 10000.0
epsilon = 1e-06


def nothing_yet(value, identity):
    return jax.tree.map(
        lambda part, zero: jnp.zeros_like(part) + jnp.asarray(zero, part.dtype), value, identity
    )


def collected_together(value, axis):
    leaves = jax.tree.leaves(value)
    sequence = sorted(range(len(leaves)), key=lambda k: -leaves[k].size)
    width = (1, *leaves[sequence[0]].shape)[-1]
    lines = [
        jnp.pad(leaves[k].reshape(-1), (0, -leaves[k].size % width)).reshape(-1, width)
        for k in sequence
    ]
    both, at, found = (lax.all_gather(jnp.concatenate(lines), axis), 0, {})
    for k, line in zip(sequence, lines):
        slab = both[:, at : at + len(line)].reshape(len(both), -1)
        found[k] = slab[:, : leaves[k].size].reshape(-1, *leaves[k].shape)
        at += len(line)
    numbers = iter(range(len(leaves)))
    return jax.tree.map(lambda _: found[next(numbers)], value)


def prefix_by_axis(value, axes, combine, identity):
    before = start = nothing_yet(value, identity)
    total = value
    for axis in reversed(axes):
        count, here = (lax.axis_size(axis), lax.axis_index(axis))
        pieces = collected_together(
            jax.tree.map(
                lambda part, kind: part.astype(kind),
                total,
                (jnp.bfloat16, jnp.bfloat16, jnp.bfloat16, jnp.bfloat16),
            ),
            axis,
        )
        inside, total = (start, start)
        for k in range(count):
            passed = k < here
            total = combine(
                total, jax.tree.map(lambda part, own: part[k].astype(own.dtype), pieces, value)
            )
            inside = jax.tree.map(lambda new, old: jnp.where(passed, new, old), total, inside)
        before = combine(inside, before)
    return before


def rotate(payload_tensor, positions):
    channel_dimension = payload_tensor.shape[-1]
    half = channel_dimension // 2
    freq = rope_base ** (-jnp.arange(half, dtype=jnp.float32) * 2.0 / channel_dimension)
    angle = positions.astype(jnp.float32)[:, None, None] * freq[None, None, :]
    cosine = jnp.cos(angle)
    sine = jnp.sin(angle)
    first = payload_tensor[..., :half]
    second = payload_tensor[..., half:]
    return jnp.concatenate([first * cosine - second * sine, first * sine + second * cosine], -1)


def segment_terms(probe_tensor, lookup_tensor, payload_tensor, surge_forgetting, forgetting_speed):
    length = probe_tensor.shape[0]
    segment_tally = jnp.arange(length, dtype=jnp.float32)
    memory_matrix = (
        forgetting_speed[None, :] * segment_tally[:, None] + jnp.cumsum(surge_forgetting)[:, None]
    )
    causal = (segment_tally[:, None] >= segment_tally[None, :])[None]
    level_t = jnp.transpose(memory_matrix)
    gap = level_t[:, :, None] - level_t[:, None, :]
    decay = jnp.where(causal, jnp.exp(jnp.where(causal, gap, 0.0)), 0.0)
    attention_scores = jnp.einsum(
        "szr,yzr->zsy", probe_tensor, lookup_tensor, preferred_element_type=jnp.float32
    )
    weights = (attention_scores * decay).astype(jnp.bfloat16)
    inner = jnp.einsum("htm,mhe->the", weights, payload_tensor, preferred_element_type=jnp.float32)
    factor = jnp.exp(memory_matrix + forgetting_speed[None, :])
    tail = jnp.exp(memory_matrix[-1:, :] - memory_matrix)
    weighted_output = (lookup_tensor.astype(jnp.float32) * tail[:, :, None]).astype(jnp.bfloat16)
    state_update = jnp.einsum(
        "oup,our->upr", weighted_output, payload_tensor, preferred_element_type=jnp.float32
    )
    total = jnp.exp(memory_matrix[-1] + forgetting_speed)
    return (inner, factor, state_update, total)


def read_state(probe_tensor, state):
    return jnp.einsum("thd,hde->the", probe_tensor.astype(jnp.float32), state)


def keeping_multiplier(
    probe_source,
    lookup_tensor,
    payload_tensor,
    forgetting_speed,
    surge_forgetting,
    channel_dimension,
    segment_begin,
):
    length = probe_source.shape[0]
    heads = probe_source.shape[1] // channel_dimension
    places = segment_begin + jnp.arange(length, dtype=jnp.int32)
    spun_probe = rotate(
        probe_source.astype(jnp.float32).reshape(length, heads, channel_dimension), places
    ).astype(jnp.bfloat16)
    spun_lookup = (
        rotate(lookup_tensor.astype(jnp.float32).reshape(length, heads, channel_dimension), places)
        * channel_dimension ** (-0.5)
    ).astype(jnp.bfloat16)
    regrouped_payload = payload_tensor.reshape(length, heads, channel_dimension)
    block = min(512, length)
    count = length // block

    def divider_mark(array):
        return array.reshape((count, block) + array.shape[1:])

    def segment_walker(carry, piece):
        state, prefix = carry
        block_q, block_k, block_v, block_b = piece
        inner, factor, state_update, total = segment_terms(
            block_q, block_k, block_v, block_b, forgetting_speed
        )
        local = inner + factor[:, :, None] * read_state(block_q, state)
        return (
            (total[:, None, None] * state + state_update, prefix * total),
            (local, factor * prefix[None, :]),
        )

    opening_location = (
        jnp.zeros((heads, channel_dimension, channel_dimension), jnp.float32),
        jnp.ones((heads,), jnp.float32),
    )
    (state, decay), (local, reach) = lax.scan(
        segment_walker,
        opening_location,
        (
            divider_mark(spun_probe),
            divider_mark(spun_lookup),
            divider_mark(regrouped_payload),
            divider_mark(surge_forgetting),
        ),
    )
    return (
        spun_probe,
        local.reshape(length, heads, channel_dimension),
        reach.reshape(length, heads),
        decay,
        state,
    )


def finish(sublayer_final, emission_valve, scaling_coefficients):
    length, heads, channel_dimension = sublayer_final.shape
    normed = sublayer_final * lax.rsqrt(
        jnp.mean(sublayer_final * sublayer_final, -1, keepdims=True) + epsilon
    )
    gated = (
        normed.reshape(length, heads * channel_dimension)
        * scaling_coefficients[None, :]
        * jax.nn.silu(emission_valve.astype(jnp.float32))
    )
    return gated.astype(jnp.bfloat16)


def chain(earlier, later):
    return (
        earlier[0] * later[0],
        later[0][:, None, None] * earlier[1] + later[1],
        earlier[2] * later[2],
        later[2][:, None, None] * earlier[3] + later[3],
    )


def slot_positions(chosen, experts, cap):
    listed = chosen.reshape(-1)
    matches = (listed[:, None] == jnp.arange(experts, dtype=jnp.int32)[None, :]).astype(jnp.int32)
    before = jnp.cumsum(matches, 0) - matches
    order = jnp.sum(before * matches, 1)
    return (listed * cap + order).reshape(chosen.shape)


def fill_slots(rows_in, chosen, experts, cap):
    count = rows_in.shape[0]
    places = slot_positions(chosen, experts, cap).reshape(-1)
    owners = jnp.repeat(jnp.arange(count, dtype=jnp.int32), 2)
    source = jnp.full((experts * cap,), count, jnp.int32).at[places].set(owners)
    padded = jnp.concatenate([rows_in, jnp.zeros((1, rows_in.shape[1]), rows_in.dtype)], 0)
    return padded[source].reshape(experts, cap, rows_in.shape[1])


def on_device(
    broad_probe_tensor,
    broad_lookup_tensor,
    broad_payload_tensor,
    broad_emission_valve,
    slim_probe_tensor,
    slim_lookup_tensor,
    slim_payload_tensor,
    slim_emission_valve,
    broad_forgetting_speed,
    slim_forgetting_speed,
    broad_channel_scaling,
    slim_channel_scaling,
    surge_forgetting,
    broad_emission_proj,
    slim_emission_proj,
    skip_stream,
    premix_scaling_coeffs,
    routed_specialist_ids,
    routed_specialist_shares,
    specialist_valve_proj,
    specialist_expand_proj,
    specialist_contract_proj,
):
    length = broad_probe_tensor.shape[0]
    segment_begin = lax.axis_index(SP) * length
    wide_result = keeping_multiplier(
        broad_probe_tensor,
        broad_lookup_tensor,
        broad_payload_tensor,
        broad_forgetting_speed,
        surge_forgetting,
        BROAD_CHANNEL_DIM,
        segment_begin,
    )
    narrow_result = keeping_multiplier(
        slim_probe_tensor,
        slim_lookup_tensor,
        slim_payload_tensor,
        slim_forgetting_speed,
        surge_forgetting,
        THIN_CHANNEL_DIM,
        segment_begin,
    )
    identity = (
        jnp.ones_like(wide_result[3]),
        jnp.zeros_like(wide_result[4]),
        jnp.ones_like(narrow_result[3]),
        jnp.zeros_like(narrow_result[4]),
    )
    incoming = prefix_by_axis(
        (wide_result[3], wide_result[4], narrow_result[3], narrow_result[4]), SP, chain, identity
    )
    mixed_wide = finish(
        wide_result[1] + wide_result[2][:, :, None] * read_state(wide_result[0], incoming[1]),
        broad_emission_valve,
        broad_channel_scaling,
    )
    mixed_narrow = finish(
        narrow_result[1] + narrow_result[2][:, :, None] * read_state(narrow_result[0], incoming[3]),
        slim_emission_valve,
        slim_channel_scaling,
    )
    rows_wide, rows_narrow = (
        lax.all_to_all(mixed_wide, "tp", split_axis=0, concat_axis=1, tiled=True),
        lax.all_to_all(mixed_narrow, "tp", split_axis=0, concat_axis=1, tiled=True),
    )
    projected = jnp.dot(rows_wide, broad_emission_proj, preferred_element_type=jnp.float32)
    projected = projected + jnp.dot(
        rows_narrow, slim_emission_proj, preferred_element_type=jnp.float32
    )
    updated = skip_stream.astype(jnp.float32) + projected
    scale = lax.rsqrt(jnp.mean(updated * updated, -1, keepdims=True) + epsilon)
    normed = (updated * scale * premix_scaling_coeffs[None, :]).astype(jnp.bfloat16)
    rows = normed.shape[0]
    width = normed.shape[1]
    experts = lax.axis_size(SP) * specialist_valve_proj.shape[0]
    cap = rows * GROUPS // experts
    own_ids = lax.dynamic_slice_in_dim(routed_specialist_ids, lax.axis_index("tp") * rows, rows, 0)
    own_weights = lax.dynamic_slice_in_dim(
        routed_specialist_shares, lax.axis_index("tp") * rows, rows, 0
    )
    own_places = slot_positions(own_ids, experts, cap)
    sent = lax.all_to_all(
        fill_slots(normed, own_ids, experts, cap), SP, split_axis=0, concat_axis=0, tiled=True
    )
    arrived = lax.all_gather(sent, "tp", axis=0, tiled=True)
    slots = arrived.reshape(-1, width)
    emission_valve = jnp.dot(slots, specialist_valve_proj[0], preferred_element_type=jnp.float32)
    up = jnp.dot(slots, specialist_expand_proj[0], preferred_element_type=jnp.float32)
    hidden = (jax.nn.silu(emission_valve) * up).astype(jnp.bfloat16)
    summed = lax.psum_scatter(
        jnp.dot(hidden, specialist_contract_proj[0], preferred_element_type=jnp.float32).astype(
            jnp.bfloat16
        ),
        "tp",
        scatter_dimension=0,
        tiled=True,
    )
    expert_out = summed.reshape(experts, cap, width)
    returned = lax.all_to_all(expert_out, SP, split_axis=0, concat_axis=0, tiled=True)
    picked = returned.reshape(experts * cap, width)[own_places]
    mixture = jnp.sum(own_weights[:, :, None] * picked.astype(jnp.float32), 1)
    return (updated + mixture).astype(jnp.bfloat16)


def solution(mesh):
    finer = Mesh(mesh.devices.reshape(8, 4, mesh.shape["tp"]), ("sp_0", "sp_1", "tp"))
    return jax.shard_map(
        on_device,
        mesh=finer,
        in_specs=(
            P(SP, "tp"),
            P(SP, "tp"),
            P(SP, "tp"),
            P(SP, "tp"),
            P(SP, "tp"),
            P(SP, "tp"),
            P(SP, "tp"),
            P(SP, "tp"),
            P("tp"),
            P("tp"),
            P("tp"),
            P("tp"),
            P(SP),
            P(),
            P(),
            P(SP_TP, None),
            P(),
            P(SP, None),
            P(SP, None),
            P(SP, None, "tp"),
            P(SP, None, "tp"),
            P(SP, "tp", None),
        ),
        out_specs=P(SP_TP, None),
        check_vma=False,
    )
```

profile of v0, /device:TPU:2, one launch (start us, length us, event | category | flops | bytes accessed | tf_op | source)
XLA Modules:
  0.0 307.2 jit_solution(5164450144786927147)
XLA Ops:
  6.6 1.1 reduce-window.9
  7.7 0.1 slice_reduce_fusion
  7.9 0.7 multiply_add_fusion.2
  8.7 0.2 slice_reduce_fusion.1
  8.9 0.7 add_exponential_fusion
  9.6 0.7 broadcast_multiply_fusion.2
  10.3 1.0 copy.137
  11.4 1.0 copy.146
  12.4 1.0 copy.138
  13.4 0.3 multiply_cosine_fusion.1
  13.8 0.2 fusion.27
  14.0 0.1 reshape.1113
  14.1 0.6 slice.349
  16.1 1.3 fusion.80
  17.4 0.1 fusion.68
  17.6 0.3 fusion.26
  18.0 12.2 %all-gather.2 = bf16[4,194,128]{2,1,0:T(8,128)(2,1)S(1)} all-gather(bf16[1,194,128]{2,1,0:T(8,128)(2,1)S(1)} %maximum_bitcast_fusion), channel_id=2, replica_groups=mesh['sp_0'=8,'sp_1'=4,'tp'=8] {'sp_1'}, dimensions={0}, use_global_device_ids=true | all-gather | bytes 248320 | tf_op jit(solution)/shard_map/all_gather | solution.py:30
  30.2 0.6 fusion.258
  34.9 28.8 %all-gather.3 = bf16[8,194,128]{2,1,0:T(8,128)(2,1)S(1)} all-gather(bf16[1,194,128]{2,1,0:T(8,128)(2,1)S(1)} %maximum_bitcast_fusion.1), channel_id=3, replica_groups=mesh['sp_0'=8,'sp_1'=4,'tp'=8] {'sp_0'}, dimensions={0}, use_global_device_ids=true | all-gather | bytes 446976 | tf_op jit(solution)/shard_map/all_gather | solution.py:30
  63.7 0.6 fusion.257
  70.1 0.6 fusion.20
  70.7 0.3 fusion.25
  71.0 0.4 multiply_reduce_fusion.3
  71.4 0.8 fusion.71
  72.2 4.5 %all-to-all-start = ((bf16[8,64,128]{2,1,0:T(8,128)(2,1)}), bf16[8,64,128]{2,1,0:T(8,128)(2,1)S(1)}, u32[]{:S(2)}, u32[]{:S(2)}) async-start(bf16[8,64,128]{2,1,0:T(8,128)(2,1)} %bitcast.66), calls=%async_computation | async-start | bytes 262144 | tf_op jit(solution)/shard_map/all_to_all | solution.py:268
  76.8 0.2 iota_compare_fusion
  77.3 0.1 copy.149
  77.6 0.1 copy.151
  79.1 1.1 fusion.21
  80.2 0.2 fusion.19
  80.4 0.3 multiply_reduce_fusion.2
  80.8 0.1 copy.160
  80.9 0.8 constant_dynamic-slice_fusion
  81.7 0.1 copy.170
  81.8 0.1 eq.8
  81.9 0.1 fusion.82
  82.0 0.2 reduce_window_sum.66
  82.2 0.2 select_reduce_fusion
  82.3 0.1 reduce_sum.58
  82.5 0.1 mul.995
  82.7 0.1 reshape.1196
  82.8 1.0 scatter_custom_fusion
  83.8 0.7 fusion.70
  84.6 4.8 %all-to-all-start.1 = ((bf16[8,64,128]{2,1,0:T(8,128)(2,1)}), bf16[8,64,128]{2,1,0:T(8,128)(2,1)S(1)}, u32[]{:S(2)}, u32[]{:S(2)}) async-start(bf16[8,64,128]{2,1,0:T(8,128)(2,1)} %bitcast.82), calls=%async_computation.1 | async-start | bytes 262144 | tf_op jit(solution)/shard_map/all_to_all | solution.py:269
  89.4 3.1 fusion.74
  92.5 3.0 all-to-all-done.1
  95.5 3.2 %multiply_reduce_fusion.1 = (f32[64]{0:T(128)S(1)}, f32[64,2048]{1,0:T(8,128)S(1)}) fusion(f32[64,2048]{1,0:T(8,128)S(1)} %fusion.74, bf16[1024,2048]{1,0:T(8,128)(2,1)} %param.36, bf16[64,2048]{1,0:T(8,128)(2,1)S(1)} %copy-done.1, bf16[8,64,128]{2,1,0:T(8,128)(2,1)S(1)} %all-to-all-done.1), kind=kOutput, calls=%fused_computation.51 | convolution fusion | flops 269090752 | bytes 5636352 | tf_op jit(solution)/shard_map/dot_general | solution.py:272
  98.7 0.1 multiply_convert_fusion.1
  98.9 1.4 gather_fusion
  100.2 35.5 %all_to_all.48 = bf16[32,8,2048]{2,1,0:T(8,128)(2,1)} all-to-all(bf16[32,8,2048]{2,1,0:T(8,128)(2,1)S(1)} %bitcast.268), channel_id=1, replica_groups=mesh['sp_0'=8,'sp_1'=4,'tp'=8] {'sp_0','sp_1'}, dimensions={0} | all-to-all | bytes 2097152 | tf_op jit(solution)/shard_map/all_to_all | solution.py:287
  135.8 0.2 reduce-scatter.2.cloned.1.call-start
  136.0 47.0 %all-gather.6.cloned.1.call-done = bf16[256,8,2048]{2,1,0:T(8,128)(2,1)} async-done(((bf16[32,8,2048]{2,1,0:T(8,128)(2,1)}), bf16[256,8,2048]{2,1,0:T(8,128)(2,1)}) %all-gather.6.cloned.1.call-update) | async-done | bytes 8388624 | tf_op jit(solution)/shard_map/all_gather | solution.py:290
  183.0 7.3 %fusion.2 = f32[2048,256]{1,0:T(8,128)} fusion(bf16[256,8,2048]{2,1,0:T(8,128)(2,1)} %all-gather.6.cloned.1.call-done, bf16[1,2048,256]{2,1,0:T(8,128)(2,1)} %param.41), kind=kOutput, calls=%fused_computation.5 | convolution fusion | flops 2147483648 | bytes 11534336 | tf_op jit(solution)/shard_map/dot_general | solution.py:292
  190.3 13.1 %convolution_convert_fusion = bf16[2048,2048]{1,0:T(8,128)(2,1)} fusion(bf16[256,8,2048]{2,1,0:T(8,128)(2,1)} %all-gather.6.cloned.1.call-done, f32[2048,256]{1,0:T(8,128)} %fusion.2, bf16[1,256,2048]{2,1,0:T(8,128)(2,1)S(1)} %copy-done, bf16[1,2048,256]{2,1,0:T(8,128)(2,1)S(1)} %copy-done.10), kind=kOutput, calls=%fused_computation.7 | convolution fusion | flops 4302307328 | bytes 20971520 | tf_op jit(solution)/shard_map/dot_general | solution.py:296
  203.4 55.4 %reduce-scatter.2.cloned.1.call-done = bf16[256,2048]{1,0:T(8,128)(2,1)} async-done(((bf16[2048,2048]{1,0:T(8,128)(2,1)}), bf16[256,2048]{1,0:T(8,128)(2,1)}) %reduce-scatter.2.cloned.1.call-update) | async-done | bytes 1048592 | tf_op jit(solution)/shard_map/reduce_scatter | solution.py:295
  258.8 10.1 %all-to-all-start.3 = ((bf16[32,8,2048]{2,1,0:T(8,128)(2,1)}), bf16[32,8,2048]{2,1,0:T(8,128)(2,1)S(1)}, u32[]{:S(2)}, u32[]{:S(2)}) async-start(bf16[32,8,2048]{2,1,0:T(8,128)(2,1)} %bitcast.269), calls=%async_computation.4 | async-start | bytes 2097152 | tf_op jit(solution)/shard_map/all_to_all | solution.py:304
  269.0 0.1 reshape.1186
  269.1 0.8 constant_dynamic-slice_fusion.1
  269.9 0.1 copy.162
  270.0 26.5 %all-to-all-done.3 = bf16[32,8,2048]{2,1,0:T(8,128)(2,1)S(1)} async-done(((bf16[32,8,2048]{2,1,0:T(8,128)(2,1)}), bf16[32,8,2048]{2,1,0:T(8,128)(2,1)S(1)}, u32[]{:S(2)}, u32[]{:S(2)}) %all-to-all-start.3) | async-done | bytes 1048608 | tf_op jit(solution)/shard_map/all_to_all | solution.py:304
  296.5 0.9 gather_fusion.1
  297.4 0.7 reshape.1205
  298.1 1.5 multiply_reduce_fusion
  299.6 0.8 add_convert_fusion
  (101 shorter events, 3.3 us)
Async XLA Ops:
  6.5 183.8 %copy-start = (bf16[1,256,2048]{2,1,0:T(8,128)(2,1)S(1)}, bf16[1,256,2048]{2,1,0:T(8,128)(2,1)}, u32[]{:S(2)}) copy-start(bf16[1,256,2048]{2,1,0:T(8,128)(2,1)} %param.43) | copy-start | bytes 3145732
  6.5 9.5 %copy-start.5 = (bf16[512,128]{1,0:T(8,128)(2,1)S(1)}, bf16[512,128]{1,0:T(8,128)(2,1)}, u32[]{:S(2)}) copy-start(bf16[512,128]{1,0:T(8,128)(2,1)} %param.22) | copy-start | bytes 393220
  6.5 9.5 %copy-start.4 = (bf16[512,128]{1,0:T(8,128)(2,1)S(1)}, bf16[512,128]{1,0:T(8,128)(2,1)}, u32[]{:S(2)}) copy-start(bf16[512,128]{1,0:T(8,128)(2,1)} %param.23) | copy-start | bytes 393220
  13.8 3.8 %copy-start.11 = (bf16[512,128]{1,0:T(8,128)(2,1)S(1)}, bf16[512,128]{1,0:T(8,128)(2,1)}, u32[]{:S(2)}) copy-start(bf16[512,128]{1,0:T(8,128)(2,1)} %param.24) | copy-start | bytes 393220
  70.1 1.3 copy-start.2
  70.1 1.3 copy-start.8
  70.7 6.1 %copy-start.7 = (f32[2]{0:T(128)S(1)}, f32[2]{0:T(128)}, u32[]{:S(2)}) copy-start(f32[2]{0:T(128)} %param.31) | copy-start | bytes 28
  72.2 12.4 %all-to-all-start = ((bf16[8,64,128]{2,1,0:T(8,128)(2,1)}), bf16[8,64,128]{2,1,0:T(8,128)(2,1)S(1)}, u32[]{:S(2)}, u32[]{:S(2)}) async-start(bf16[8,64,128]{2,1,0:T(8,128)(2,1)} %bitcast.66), calls=%async_computation | async-start | bytes 262144 | tf_op jit(solution)/shard_map/all_to_all | solution.py:268
  80.2 3.6 %copy-start.3 = (bf16[512,128]{1,0:T(8,128)(2,1)S(1)}, bf16[512,128]{1,0:T(8,128)(2,1)}, u32[]{:S(2)}) copy-start(bf16[512,128]{1,0:T(8,128)(2,1)} %param.29) | copy-start | bytes 393220
  80.2 3.6 %copy-start.9 = (f32[128]{0:T(128)S(1)}, f32[128]{0:T(128)}, u32[]{:S(2)}) copy-start(f32[128]{0:T(128)} %param.33) | copy-start | bytes 1540
  84.6 10.9 %all-to-all-start.1 = ((bf16[8,64,128]{2,1,0:T(8,128)(2,1)}), bf16[8,64,128]{2,1,0:T(8,128)(2,1)S(1)}, u32[]{:S(2)}, u32[]{:S(2)}) async-start(bf16[8,64,128]{2,1,0:T(8,128)(2,1)} %bitcast.82), calls=%async_computation.1 | async-start | bytes 262144 | tf_op jit(solution)/shard_map/all_to_all | solution.py:269
  89.4 6.1 %copy-start.1 = (bf16[64,2048]{1,0:T(8,128)(2,1)S(1)}, bf16[64,2048]{1,0:T(8,128)(2,1)}, u32[]{:S(2)}) copy-start(bf16[64,2048]{1,0:T(8,128)(2,1)} %param.37) | copy-start | bytes 786436
  89.4 93.6 %all-gather.6.cloned.1.call-start = ((), (), s32[]{:S(2)}) async-start(), calls=%async_computation.5 | async-start | bytes 9437184 | tf_op jit(solution)/shard_map/all_gather | solution.py:290
  92.5 6.2 %copy-start.6 = (f32[2048]{0:T(1024)S(1)}, f32[2048]{0:T(1024)}, u32[]{:S(2)}) copy-start(f32[2048]{0:T(1024)} %param.38) | copy-start | bytes 24580
  135.7 54.6 %copy-start.10 = (bf16[1,2048,256]{2,1,0:T(8,128)(2,1)S(1)}, bf16[1,2048,256]{2,1,0:T(8,128)(2,1)}, u32[]{:S(2)}) copy-start(bf16[1,2048,256]{2,1,0:T(8,128)(2,1)} %param.42) | copy-start | bytes 3145732
  135.8 123.1 %reduce-scatter.2.cloned.1.call-start = ((), (), s32[]{:S(2)}) async-start(), calls=%async_computation.6 | async-start | bytes 9437184 | tf_op jit(solution)/shard_map/reduce_scatter | solution.py:295
  258.8 37.6 %all-to-all-start.3 = ((bf16[32,8,2048]{2,1,0:T(8,128)(2,1)}), bf16[32,8,2048]{2,1,0:T(8,128)(2,1)S(1)}, u32[]{:S(2)}, u32[]{:S(2)}) async-start(bf16[32,8,2048]{2,1,0:T(8,128)(2,1)} %bitcast.269), calls=%async_computation.4 | async-start | bytes 2097152 | tf_op jit(solution)/shard_map/all_to_all | solution.py:304
Sparse Core Ops, SparseCore 0:
  135.9 47.0 all-gather.5
  203.6 55.2 reduce-scatter.1
where the time goes:
time: 308 us; the launch traced here: 307 us
  waiting for transfers between devices  132 us (43%)
  blocking collectives  76.5 us (25%)
  matrix products  30.1 us (10%)
  between operations  24.4 us (8%)
  starting transfers between devices  19.7 us (6%)
  local copies, waits for them, and re-layouts  14.4 us (5%)
  other arithmetic  10.2 us (3%)
    reduce_scatter x1, waiting for transfers between devices, on_device(): lax.psum_scatter(jnp.dot(hidden, specialist_contract_proj[0], preferred_e...  55.4 us
    all_gather x1, waiting for transfers between devices, on_device(): arrived = lax.all_gather(sent, 'tp', axis=0, tiled=True)  47 us
    all_gather x2, blocking collectives, collected_together(): both, at, found = (lax.all_gather(jnp.concatenate(lines), axis), 0, {})  41 us
    all_to_all x1, blocking collectives, on_device(): lax.all_to_all(fill_slots(normed, own_ids, experts, cap), SP, split_axis=...  35.5 us
    all_to_all x1, waiting for transfers between devices, on_device(): lax.all_to_all(expert_out, SP, split_axis=0, concat_axis=0, tiled=True)  26.5 us
    dot_general x1, matrix products, on_device(): jnp.dot(hidden, specialist_contract_proj[0], preferred_element_type=jnp.f...  13.1 us
    all_to_all x1, starting transfers between devices, on_device(): lax.all_to_all(expert_out, SP, split_axis=0, concat_axis=0, tiled=True)  10.1 us
    dot_general x1, matrix products, on_device(): jnp.dot(slots, specialist_valve_proj[0], preferred_element_type=jnp.float32)  7.3 us
  transfers between devices with their start and end apart: 5, of which 4 were waited for; matrix products, arithmetic and copies ran while one was open for 4% of the time, Pallas kernels for 0%

commit v1 on v0

--- a/solution.py
+++ b/solution.py
@@ -287,7 +287,8 @@
     sent = lax.all_to_all(
         fill_slots(normed, own_ids, experts, cap), SP, split_axis=0, concat_axis=0, tiled=True
     )
-    arrived = lax.all_gather(sent, "tp", axis=0, tiled=True)
+    outgoing = jnp.stack([sent] * lax.axis_size("tp"))
+    arrived = jnp.concatenate(lax.all_to_all(outgoing, "tp", 0, 0), axis=0)
     slots = arrived.reshape(-1, width)
     emission_valve = jnp.dot(slots, specialist_valve_proj[0], preferred_element_type=jnp.float32)
     up = jnp.dot(slots, specialist_expand_proj[0], preferred_element_type=jnp.float32)

time: 308 us -> 357 us (1.16)
  blocking collectives: 76.5 us -> 174 us
  waiting for transfers between devices: 132 us -> 80.1 us
  local copies, waits for them, and re-layouts: 14.4 us -> 18.6 us
    all_to_all x0 -> x1, blocking collectives: none -> 97.3 us  [on_device(): arrived = jnp.concatenate(lax.all_to_all(outgoing, 'tp', 0, 0), axis=0)]
    all_gather x1 -> x0, waiting for transfers between devices: 47 us -> none  [on_device(): arrived = lax.all_gather(sent, 'tp', axis=0, tiled=True)]
    reduce_scatter x1, waiting for transfers between devices: 55.4 us -> 50.6 us  [on_device(): lax.psum_scatter(jnp.dot(hidden, specialist_contract_proj[0], preferred_e...]
    dot_general x1, matrix products: 13.1 us -> 16.8 us  [on_device(): jnp.dot(hidden, specialist_contract_proj[0], preferred_element_type=jnp.f...]
  transfers between devices with their start and end apart: 5 -> 4, of which waited for: 4 -> 3; matrix products, arithmetic and copies ran while one was open for 4% -> 3% of each run, Pallas kernels for 0% -> 0%
where the time goes in v1:
time: 357 us; the launch traced here: 356 us
  blocking collectives  174 us (49%)
  waiting for transfers between devices  80.1 us (22%)
  matrix products  30.2 us (8%)
  between operations  24.1 us (7%)
  starting transfers between devices  19.5 us (5%)
  local copies, waits for them, and re-layouts  18.6 us (5%)
  other arithmetic  10.2 us (3%)
    all_to_all x1, blocking collectives, on_device(): arrived = jnp.concatenate(lax.all_to_all(outgoing, 'tp', 0, 0), axis=0)  97.3 us
    reduce_scatter x1, waiting for transfers between devices, on_device(): lax.psum_scatter(jnp.dot(hidden, specialist_contract_proj[0], preferred_e...  50.6 us
    all_gather x2, blocking collectives, collected_together(): both, at, found = (lax.all_gather(jnp.concatenate(lines), axis), 0, {})  41 us
    all_to_all x1, blocking collectives, on_device(): lax.all_to_all(fill_slots(normed, own_ids, experts, cap), SP, split_axis=...  35.4 us
    all_to_all x1, waiting for transfers between devices, on_device(): lax.all_to_all(expert_out, SP, split_axis=0, concat_axis=0, tiled=True)  26.5 us
    dot_general x1, matrix products, on_device(): jnp.dot(hidden, specialist_contract_proj[0], preferred_element_type=jnp.f...  16.8 us
    all_to_all x1, starting transfers between devices, on_device(): lax.all_to_all(expert_out, SP, split_axis=0, concat_axis=0, tiled=True)  10.1 us
  transfers between devices with their start and end apart: 4, of which 3 were waited for; matrix products, arithmetic and copies ran while one was open for 3% of the time, Pallas kernels for 0%

profile of v1, /device:TPU:2, one launch (start us, length us, event | category | flops | bytes accessed | tf_op | source)
XLA Modules:
  0.0 356.4 jit_solution(7474743858232897169)
XLA Ops:
  6.6 1.1 reduce-window.9
  7.7 0.1 slice_reduce_fusion
  7.9 0.7 multiply_add_fusion.2
  8.7 0.2 slice_reduce_fusion.1
  8.9 0.7 add_exponential_fusion
  9.6 0.7 broadcast_multiply_fusion.2
  10.3 1.0 copy.137
  11.4 1.0 copy.146
  12.4 1.0 copy.138
  13.4 0.3 multiply_cosine_fusion.1
  13.8 0.2 fusion.16
  14.0 0.1 reshape.1112
  14.1 0.6 slice.349
  16.0 1.3 fusion.70
  17.3 0.1 fusion.58
  17.5 0.3 fusion.15
  17.9 12.2 %all-gather.2 = bf16[4,194,128]{2,1,0:T(8,128)(2,1)S(1)} all-gather(bf16[1,194,128]{2,1,0:T(8,128)(2,1)S(1)} %maximum_bitcast_fusion), channel_id=2, replica_groups=mesh['sp_0'=8,'sp_1'=4,'tp'=8] {'sp_1'}, dimensions={0}, use_global_device_ids=true | all-gather | bytes 248320 | tf_op jit(solution)/shard_map/all_gather | solution.py:30
  30.1 0.6 fusion.248
  34.6 28.8 %all-gather.3 = bf16[8,194,128]{2,1,0:T(8,128)(2,1)S(1)} all-gather(bf16[1,194,128]{2,1,0:T(8,128)(2,1)S(1)} %maximum_bitcast_fusion.1), channel_id=3, replica_groups=mesh['sp_0'=8,'sp_1'=4,'tp'=8] {'sp_0'}, dimensions={0}, use_global_device_ids=true | all-gather | bytes 446976 | tf_op jit(solution)/shard_map/all_gather | solution.py:30
  63.4 0.6 fusion.247
  69.7 0.6 fusion.9
  70.3 0.3 fusion.14
  70.6 0.4 multiply_reduce_fusion.3
  71.0 0.8 fusion.61
  71.8 4.5 %all-to-all-start = ((bf16[8,64,128]{2,1,0:T(8,128)(2,1)}), bf16[8,64,128]{2,1,0:T(8,128)(2,1)S(1)}, u32[]{:S(2)}, u32[]{:S(2)}) async-start(bf16[8,64,128]{2,1,0:T(8,128)(2,1)} %bitcast.66), calls=%async_computation | async-start | bytes 262144 | tf_op jit(solution)/shard_map/all_to_all | solution.py:268
  76.4 0.2 iota_compare_fusion
  76.7 0.1 copy.148
  78.6 1.1 fusion.10
  79.8 0.2 fusion.8
  80.0 0.3 multiply_reduce_fusion.2
  80.4 0.1 copy.160
  80.5 0.8 constant_dynamic-slice_fusion
  81.2 0.1 copy.170
  81.3 0.1 eq.8
  81.5 0.1 fusion.72
  81.6 0.2 reduce_window_sum.66
  81.8 0.2 select_reduce_fusion
  81.9 0.1 reduce_sum.58
  82.1 0.1 mul.995
  82.3 0.1 reshape.1194
  82.4 1.0 scatter_custom_fusion
  83.4 0.7 fusion.60
  84.2 4.8 %all-to-all-start.1 = ((bf16[8,64,128]{2,1,0:T(8,128)(2,1)}), bf16[8,64,128]{2,1,0:T(8,128)(2,1)S(1)}, u32[]{:S(2)}, u32[]{:S(2)}) async-start(bf16[8,64,128]{2,1,0:T(8,128)(2,1)} %bitcast.82), calls=%async_computation.1 | async-start | bytes 262144 | tf_op jit(solution)/shard_map/all_to_all | solution.py:269
  89.0 3.1 fusion.64
  92.1 3.0 all-to-all-done.1
  95.1 3.2 multiply_reduce_fusion.1
  98.3 0.1 multiply_convert_fusion.1
  98.4 1.4 gather_fusion
  99.8 35.4 %all_to_all.53 = bf16[32,8,2048]{2,1,0:T(8,128)(2,1)S(1)} all-to-all(bf16[32,8,2048]{2,1,0:T(8,128)(2,1)S(1)} %bitcast.262), channel_id=1, replica_groups=mesh['sp_0'=8,'sp_1'=4,'tp'=8] {'sp_0','sp_1'}, dimensions={0} | all-to-all | bytes 2097152 | tf_op jit(solution)/shard_map/all_to_all | solution.py:287
  135.2 1.1 stack.2
  136.3 97.3 %all_to_all.54 = bf16[8,32,8,2048]{3,2,1,0:T(8,128)(2,1)S(1)} all-to-all(bf16[8,32,8,2048]{3,2,1,0:T(8,128)(2,1)S(1)} %stack.2), channel_id=1, replica_groups=mesh['sp_0'=8,'sp_1'=4,'tp'=8] {'tp'}, dimensions={0} | all-to-all | bytes 16777216 | tf_op jit(solution)/shard_map/all_to_all | solution.py:291
  233.6 3.2 copy-done.1
  236.9 3.8 %fusion.20 = f32[2048,256]{1,0:T(8,128)} fusion(bf16[2048,2048]{1,0:T(8,128)(2,1)S(1)} %bitcast.260, bf16[1,2048,256]{2,1,0:T(8,128)(2,1)S(1)} %copy-done.11), kind=kOutput, calls=%fused_computation.33 | convolution fusion | flops 2147483648 | bytes 11534336 | tf_op jit(solution)/shard_map/dot_general | solution.py:293
  240.6 16.8 %convolution_convert_fusion = bf16[2048,2048]{1,0:T(8,128)(2,1)} fusion(bf16[2048,2048]{1,0:T(8,128)(2,1)} %bitcast.261, f32[2048,256]{1,0:T(8,128)} %fusion.20, bf16[1,256,2048]{2,1,0:T(8,128)(2,1)S(1)} %copy-done, bf16[1,2048,256]{2,1,0:T(8,128)(2,1)} %param.42), kind=kOutput, calls=%fused_computation.3 | convolution fusion | flops 4302307328 | bytes 20971520 | tf_op jit(solution)/shard_map/dot_general | solution.py:297
  257.5 50.6 %reduce-scatter.2.cloned.1.call-done = bf16[256,2048]{1,0:T(8,128)(2,1)} async-done(((bf16[2048,2048]{1,0:T(8,128)(2,1)}), bf16[256,2048]{1,0:T(8,128)(2,1)}) %reduce-scatter.2.cloned.1.call-update) | async-done | bytes 1048592 | tf_op jit(solution)/shard_map/reduce_scatter | solution.py:296
  308.1 10.1 %all-to-all-start.4 = ((bf16[32,8,2048]{2,1,0:T(8,128)(2,1)}), bf16[32,8,2048]{2,1,0:T(8,128)(2,1)S(1)}, u32[]{:S(2)}, u32[]{:S(2)}) async-start(bf16[32,8,2048]{2,1,0:T(8,128)(2,1)} %bitcast.263), calls=%async_computation.5 | async-start | bytes 2097152 | tf_op jit(solution)/shard_map/all_to_all | solution.py:305
  318.2 0.1 reshape.1184
  318.3 0.8 constant_dynamic-slice_fusion.1
  319.1 0.1 copy.162
  319.2 26.5 %all-to-all-done.4 = bf16[32,8,2048]{2,1,0:T(8,128)(2,1)S(1)} async-done(((bf16[32,8,2048]{2,1,0:T(8,128)(2,1)}), bf16[32,8,2048]{2,1,0:T(8,128)(2,1)S(1)}, u32[]{:S(2)}, u32[]{:S(2)}) %all-to-all-start.4) | async-done | bytes 1048608 | tf_op jit(solution)/shard_map/all_to_all | solution.py:305
  345.7 0.9 gather_fusion.1
  346.6 0.7 reshape.1203
  347.3 1.5 multiply_reduce_fusion
  348.8 0.8 add_convert_fusion
  (102 shorter events, 3.4 us)
Async XLA Ops:
  6.5 234.1 %copy-start = (bf16[1,256,2048]{2,1,0:T(8,128)(2,1)S(1)}, bf16[1,256,2048]{2,1,0:T(8,128)(2,1)}, u32[]{:S(2)}) copy-start(bf16[1,256,2048]{2,1,0:T(8,128)(2,1)} %param.43) | copy-start | bytes 3145732
  6.5 9.4 %copy-start.6 = (bf16[512,128]{1,0:T(8,128)(2,1)S(1)}, bf16[512,128]{1,0:T(8,128)(2,1)}, u32[]{:S(2)}) copy-start(bf16[512,128]{1,0:T(8,128)(2,1)} %param.22) | copy-start | bytes 393220
  6.5 9.4 %copy-start.5 = (bf16[512,128]{1,0:T(8,128)(2,1)S(1)}, bf16[512,128]{1,0:T(8,128)(2,1)}, u32[]{:S(2)}) copy-start(bf16[512,128]{1,0:T(8,128)(2,1)} %param.23) | copy-start | bytes 393220
  13.8 3.7 %copy-start.12 = (bf16[512,128]{1,0:T(8,128)(2,1)S(1)}, bf16[512,128]{1,0:T(8,128)(2,1)}, u32[]{:S(2)}) copy-start(bf16[512,128]{1,0:T(8,128)(2,1)} %param.24) | copy-start | bytes 393220
  69.6 1.3 copy-start.3
  69.7 1.3 copy-start.9
  70.2 6.1 %copy-start.8 = (f32[2]{0:T(128)S(1)}, f32[2]{0:T(128)}, u32[]{:S(2)}) copy-start(f32[2]{0:T(128)} %param.31) | copy-start | bytes 28
  71.8 12.4 %all-to-all-start = ((bf16[8,64,128]{2,1,0:T(8,128)(2,1)}), bf16[8,64,128]{2,1,0:T(8,128)(2,1)S(1)}, u32[]{:S(2)}, u32[]{:S(2)}) async-start(bf16[8,64,128]{2,1,0:T(8,128)(2,1)} %bitcast.66), calls=%async_computation | async-start | bytes 262144 | tf_op jit(solution)/shard_map/all_to_all | solution.py:268
  79.8 3.6 %copy-start.4 = (bf16[512,128]{1,0:T(8,128)(2,1)S(1)}, bf16[512,128]{1,0:T(8,128)(2,1)}, u32[]{:S(2)}) copy-start(bf16[512,128]{1,0:T(8,128)(2,1)} %param.29) | copy-start | bytes 393220
  79.8 3.6 %copy-start.10 = (f32[128]{0:T(128)S(1)}, f32[128]{0:T(128)}, u32[]{:S(2)}) copy-start(f32[128]{0:T(128)} %param.33) | copy-start | bytes 1540
  84.2 10.9 %all-to-all-start.1 = ((bf16[8,64,128]{2,1,0:T(8,128)(2,1)}), bf16[8,64,128]{2,1,0:T(8,128)(2,1)S(1)}, u32[]{:S(2)}, u32[]{:S(2)}) async-start(bf16[8,64,128]{2,1,0:T(8,128)(2,1)} %bitcast.82), calls=%async_computation.1 | async-start | bytes 262144 | tf_op jit(solution)/shard_map/all_to_all | solution.py:269
  89.0 6.1 %copy-start.2 = (bf16[64,2048]{1,0:T(8,128)(2,1)S(1)}, bf16[64,2048]{1,0:T(8,128)(2,1)}, u32[]{:S(2)}) copy-start(bf16[64,2048]{1,0:T(8,128)(2,1)} %param.37) | copy-start | bytes 786436
  89.0 219.1 %reduce-scatter.2.cloned.1.call-start = ((), (), s32[]{:S(2)}) async-start(), calls=%async_computation.6 | async-start | bytes 9437184 | tf_op jit(solution)/shard_map/reduce_scatter | solution.py:296
  92.1 6.2 %copy-start.7 = (f32[2048]{0:T(1024)S(1)}, f32[2048]{0:T(1024)}, u32[]{:S(2)}) copy-start(f32[2048]{0:T(1024)} %param.38) | copy-start | bytes 24580
  136.3 100.6 %copy-start.11 = (bf16[1,2048,256]{2,1,0:T(8,128)(2,1)S(1)}, bf16[1,2048,256]{2,1,0:T(8,128)(2,1)}, u32[]{:S(2)}) copy-start(bf16[1,2048,256]{2,1,0:T(8,128)(2,1)} %param.41) | copy-start | bytes 3145732
  233.6 3.2 copy-start.1
  308.1 37.6 %all-to-all-start.4 = ((bf16[32,8,2048]{2,1,0:T(8,128)(2,1)}), bf16[32,8,2048]{2,1,0:T(8,128)(2,1)S(1)}, u32[]{:S(2)}, u32[]{:S(2)}) async-start(bf16[32,8,2048]{2,1,0:T(8,128)(2,1)} %bitcast.263), calls=%async_computation.5 | async-start | bytes 2097152 | tf_op jit(solution)/shard_map/all_to_all | solution.py:305
Sparse Core Ops, SparseCore 0:
  257.6 50.4 reduce-scatter.1
